TPU v7x, 32 devices: a whole 2x2x4 slice. The times are simulated.
32 devices in a mesh: sp: 16 (over z, y, x), tp: 2 (over core).
Axes of the slice: x: 2, y: 2, z: 4, core: 2. Of those that a mesh axis runs over, the one named last changes fastest.
Arguments:
- queries: bfloat16 [3072, 1024], P('sp', 'tp'), may hold values from -6 to 6
- keys: bfloat16 [3072, 512], P('sp', 'tp'), may hold values from -6 to 6
- values: bfloat16 [3072, 512], P('sp', 'tp'), may hold values from -6 to 6
- query_gain: float32 [16, 64], P('tp'), may hold values from 1.4 to 7.5
- key_gain: float32 [8, 64], P('tp'), may hold values from 1.4 to 7.5
- out_weight: bfloat16 [1024, 2048], P('tp'), may hold values from -0.375 to 0.375
- residual: bfloat16 [3072, 2048], P('sp'), may hold values from -170 to 170
- norm_gain: float32 [2048], replicated, may hold values from 0.1 to 1.9
- gate_weight: bfloat16 [2048, 5632], P('sp', 'tp'), may hold values from -0.125 to 0.125
- up_weight: bfloat16 [2048, 5632], P('sp', 'tp'), may hold values from -0.125 to 0.125
- down_weight: bfloat16 [5632, 2048], P('tp', 'sp'), may hold values from -0.15625 to 0.15625
Outputs:
- mixed: bfloat16 [3072, 2048], P('sp')
All inputs are finite; a program needn't handle non-finite values.
Results may differ from a plain program's by a relative error of at most 0.017.
Values may be sent and summed in bfloat16 or wider, within the bound.
A program may use at most 128 MiB of HBM per device.

v0:
```python
import jax
import jax.numpy as jnp
from jax import lax
from jax.sharding import PartitionSpec as P

GRID_W = 64
epsilon = 1e-06
rope_base = 10000.0
block_keys = 2048


def rotate_pairs(entries, places):
    half = entries.shape[-1] // 2
    frequency = rope_base ** (-jnp.arange(half, dtype=jnp.float32) / half)
    angle = places.astype(jnp.float32)[:, None, None] * frequency[None, None, :]
    cosine = jnp.cos(angle)
    sine = jnp.sin(angle)
    first = entries[..., :half]
    second = entries[..., half:]
    return jnp.concatenate(
        [first * cosine - second * sine, first * sine + second * cosine], axis=-1
    )


def grid_rotate(entries, grid_rows, grid_cols):
    half = entries.shape[-1] // 2
    return jnp.concatenate(
        [
            rotate_pairs(entries[..., :half], grid_rows),
            rotate_pairs(entries[..., half:], grid_cols),
        ],
        axis=-1,
    )


def head_norm(entries, gains):
    factor = lax.rsqrt(jnp.mean(entries * entries, axis=-1, keepdims=True) + epsilon)
    return entries * factor * gains[None]


def row_norm(mid, norm_gain):
    wide = mid.astype(jnp.float32)
    return (
        wide * lax.rsqrt(jnp.mean(wide * wide, axis=-1, keepdims=True) + epsilon) * norm_gain
    ).astype(jnp.bfloat16)


def block_span(length):
    if length <= block_keys:
        return length
    span = block_keys
    while length % span != 0:
        span = span - 1
    return span


def body(
    queries,
    keys,
    values,
    query_gain,
    key_gain,
    out_weight,
    residual,
    norm_gain,
    gate_weight,
    up_weight,
    down_weight,
):
    own = queries.shape[0]
    heads = query_gain.shape[0]
    key_heads = key_gain.shape[0]
    head_size = query_gain.shape[1]
    group = heads // key_heads
    gate_full, up_full, down_full = (
        lax.all_gather(gate_weight, "sp", axis=0, tiled=True),
        lax.all_gather(up_weight, "sp", axis=0, tiled=True),
        lax.all_gather(down_weight, "sp", axis=1, tiled=True),
    )
    places = lax.axis_index("sp") * own + jnp.arange(own, dtype=jnp.int32)
    grid_rows = places // GRID_W
    grid_cols = places % GRID_W
    query_turned = grid_rotate(
        head_norm(queries.astype(jnp.float32).reshape(own, heads, head_size), query_gain),
        grid_rows,
        grid_cols,
    ).astype(jnp.bfloat16)
    query_groups = query_turned.reshape(own, key_heads, group, head_size)
    key_turned = (
        grid_rotate(
            head_norm(keys.astype(jnp.float32).reshape(own, key_heads, head_size), key_gain),
            grid_rows,
            grid_cols,
        )
        .astype(jnp.bfloat16)
        .reshape(own, key_heads * head_size)
    )
    scale = head_size ** (-0.5)

    def absorb(carry, key_block, value_block):
        top, total, summed = carry
        key_block = key_block.reshape(-1, key_heads, head_size)
        value_block = value_block.reshape(-1, key_heads, head_size)
        score = (
            jnp.einsum(
                "qgrd,kgd->qgrk", query_groups, key_block, preferred_element_type=jnp.float32
            )
            * scale
        )
        new_top = jnp.maximum(top, jnp.max(score, axis=-1))
        weight = jnp.exp(score - new_top[..., None])
        shrink = jnp.exp(top - new_top)
        total = total * shrink + jnp.sum(weight, axis=-1)
        summed = summed * shrink[..., None] + jnp.einsum(
            "qgrk,kgd->qgrd",
            weight.astype(jnp.bfloat16),
            value_block,
            preferred_element_type=jnp.float32,
        )
        return (new_top, total, summed)

    def fold_keys(carry, pieces):
        length = pieces[0].shape[0]
        span = block_span(length)
        if span == length:
            return absorb(carry, pieces[0], pieces[1])
        width = pieces[0].shape[1]
        key_blocks = pieces[0].reshape(length // span, span, width)
        value_blocks = pieces[1].reshape(length // span, span, width)

        def scan_step(inner, blocks):
            return (absorb(inner, blocks[0], blocks[1]), None)

        result, unused = lax.scan(scan_step, carry, (key_blocks, value_blocks))
        return result

    start_state = (
        jnp.full((own, key_heads, group), -jnp.inf, jnp.float32),
        jnp.zeros((own, key_heads, group), jnp.float32),
        jnp.zeros((own, key_heads, group, head_size), jnp.float32),
    )
    top, total, summed = fold_keys(
        start_state,
        (
            lax.all_gather(key_turned, "sp", axis=0, tiled=True),
            lax.all_gather(values, "sp", axis=0, tiled=True),
        ),
    )
    attended = (summed / total[..., None]).reshape(own, heads * head_size).astype(jnp.bfloat16)
    part_rows = own // lax.axis_size("tp")
    branch = lax.psum_scatter(
        jnp.dot(
            lax.slice_in_dim(attended, 0, lax.axis_size("tp") * part_rows, axis=0),
            out_weight,
            preferred_element_type=jnp.float32,
        ).astype(jnp.bfloat16),
        "tp",
        scatter_dimension=0,
        tiled=True,
    ).astype(jnp.float32)
    own_rows = lax.dynamic_slice_in_dim(residual, lax.axis_index("tp") * part_rows, part_rows, 0)
    mid = (own_rows.astype(jnp.float32) + branch).astype(jnp.bfloat16)
    normed_all = lax.all_gather(row_norm(mid, norm_gain), "tp", axis=0, tiled=True)
    gate = jnp.dot(normed_all, gate_full, preferred_element_type=jnp.float32)
    up_value = jnp.dot(normed_all, up_full, preferred_element_type=jnp.float32)
    hidden = (jax.nn.silu(gate) * up_value).astype(jnp.bfloat16)
    terms = jnp.dot(hidden, down_full, preferred_element_type=jnp.float32)
    ffn = lax.psum_scatter(
        terms.astype(jnp.bfloat16), "tp", scatter_dimension=0, tiled=True
    ).astype(jnp.float32)
    finished = (mid.astype(jnp.float32) + ffn).astype(jnp.bfloat16)
    return lax.all_gather(finished, "tp", axis=0, tiled=True)


def solution(mesh):
    in_specs = (
        P("sp", "tp"),
        P("sp", "tp"),
        P("sp", "tp"),
        P("tp", None),
        P("tp", None),
        P("tp", None),
        P("sp", None),
        P(),
        P("sp", "tp"),
        P("sp", "tp"),
        P("tp", "sp"),
    )
    out_specs = P("sp", None)
    return jax.shard_map(body, mesh=mesh, in_specs=in_specs, out_specs=out_specs, check_vma=False)
```

profile of v0, /device:TPU:0, one launch (start us, length us, event | category | flops | bytes accessed | tf_op | source)
XLA Modules:
  0.0 684.2 jit_solution(15495165526293549305)
XLA Ops:
  6.6 1.1 copy.22
  7.8 0.8 fusion.22
  8.6 0.2 multiply_cosine_fusion.1
  8.8 0.7 copy.23
  9.6 0.0 all-gather.8.cloned.1.call-start
  9.7 0.7 all-gather.8.cloned.1.call-update
  10.4 0.0 reduce-scatter.3.cloned.1.call-start
  10.4 1.1 copy.24
  11.5 0.1 fusion.19
  11.6 0.8 fusion.20
  12.4 0.1 subtract_convert_fusion.1
  12.5 0.7 pad_maximum_fusion
  13.3 57.5 %all-gather.6.cloned.1.call-done = bf16[3072,256]{1,0:T(8,128)(2,1)} async-done(((bf16[192,256]{1,0:T(8,128)(2,1)}), bf16[3072,256]{1,0:T(8,128)(2,1)}) %all-gather.6.cloned.1.call-update) | async-done | bytes 1572880 | tf_op jit(solution)/shard_map/all_gather | solution.py:145
  70.8 59.5 %all-gather.8.cloned.1.call-done = bf16[3072,256]{1,0:T(8,128)(2,1)} async-done(((bf16[192,256]{1,0:T(8,128)(2,1)}), bf16[3072,256]{1,0:T(8,128)(2,1)}) %all-gather.8.cloned.1.call-update) | async-done | bytes 1572880 | tf_op jit(solution)/shard_map/all_gather | solution.py:146
  130.3 43.6 %while.15 = (s32[]{:T(128)}, f32[192,4,2]{0,2,1:T(2,128)S(1)}, f32[192,4,2]{0,2,1:T(2,128)S(1)}, f32[192,4,2,64]{0,3,2,1:T(8,128)S(1)}, bf16[2,1536,256]{2,1,0:T...) while((s32[]{:T(128)}, f32[192,4,2]{0,2,1:T(2,128)S(1)}, ...), condition=%wide.region_5.6_spmd.clone, body=%wide.region_2.5_spmd.clone.sunk | while | flops 623156736 | bytes 37257324 | solution.py:134
  130.3 2.6 constant_dynamic-slice_fusion.3
  132.9 1.4 copy.33
  134.3 6.0 bitcast_reduce_fusion.2
  140.4 5.4 fusion.51
  145.8 1.4 copy.34
  147.2 4.8 fusion.53
  152.1 2.6 constant_dynamic-slice_fusion.3
  154.7 1.4 copy.33
  156.1 6.0 bitcast_reduce_fusion.2
  162.1 5.4 fusion.51
  167.6 1.4 copy.34
  169.0 4.8 fusion.53
  173.9 0.1 divide_convert_fusion
  173.9 1.5 convolution_convert_fusion.1
  175.4 0.0 all-gather.10.cloned.1.call-start
  175.5 0.5 all-gather.10.cloned.1.call-update
  176.0 0.0 all-gather.12.cloned.1.call-start
  176.1 0.5 all-gather.12.cloned.1.call-update
  176.7 0.5 all-gather.14.cloned.1.call-update
  177.2 0.0 reduce-scatter.5.cloned.1.call-start
  177.2 5.2 reduce-scatter.3.cloned.1.call-done
  182.5 1.4 fusion.15
  183.9 0.2 fusion.17
  184.0 2.5 all_gather.23
  186.6 141.1 %all-gather.10.cloned.1.call-done = bf16[2048,2816]{1,0:T(8,128)(2,1)} async-done(((bf16[128,2816]{1,0:T(8,128)(2,1)}), bf16[2048,2816]{1,0:T(8,128)(2,1)}) %all-gather.10.cloned.1.call-update) | async-done | bytes 11534352 | tf_op jit(solution)/shard_map/all_gather | solution.py:76
  327.6 8.0 %fusion.27 = f32[192,2816]{1,0:T(8,128)} fusion(bf16[192,2048]{1,0:T(8,128)(2,1)S(1)} %all_gather.23, bf16[2048,2816]{1,0:T(8,128)(2,1)} %all-gather.10.cloned.1.call-done), kind=kOutput, calls=%fused_computation.67 | convolution fusion | flops 2214592512 | bytes 14483456 | tf_op jit(solution)/shard_map/dot_general | solution.py:164
  335.7 134.2 %all-gather.12.cloned.1.call-done = bf16[2048,2816]{1,0:T(8,128)(2,1)} async-done(((bf16[128,2816]{1,0:T(8,128)(2,1)}), bf16[2048,2816]{1,0:T(8,128)(2,1)}) %all-gather.12.cloned.1.call-update) | async-done | bytes 11534352 | tf_op jit(solution)/shard_map/all_gather | solution.py:77
  469.9 182.8 %all-gather.14.cloned.1.call-done = bf16[2816,2048]{1,0:T(8,128)(2,1)} async-done(((bf16[2816,128]{1,0:T(8,128)(2,1)}), bf16[2816,2048]{1,0:T(8,128)(2,1)}) %all-gather.14.cloned.1.call-update) | async-done | bytes 11534352 | tf_op jit(solution)/shard_map/all_gather | solution.py:78
  652.7 13.8 %convolution_convert_fusion = bf16[192,2048]{1,0:T(8,128)(2,1)} fusion(bf16[2816,2048]{1,0:T(8,128)(2,1)} %all-gather.14.cloned.1.call-done, bf16[192,2048]{1,0:T(8,128)(2,1)S(1)} %all_gather.23, bf16[2048,2816]{1,0:T(8,128)(2,1)} %all-gather.12.cloned.1.call-done, f32[192,2816]{1,0:T(8,128)} %fusion.27), kind=kOutput, calls=%fused_computation.19 | convolution fusion | flops 4432822272 | bytes 26804224 | tf_op jit(solution)/shard_map/dot_general | solution.py:167
  666.5 6.5 reduce-scatter.5.cloned.1.call-done
  673.0 1.1 fusion.18
  674.1 2.4 all_gather.27
  676.5 0.9 copy.48
  (26 shorter events, 0.3 us)
Async XLA Ops:
  6.5 167.4 %copy-start = (bf16[512,2048]{1,0:T(8,128)(2,1)S(1)}, bf16[512,2048]{1,0:T(8,128)(2,1)}, u32[]{:S(2)}) copy-start(bf16[512,2048]{1,0:T(8,128)(2,1)} %param.18) | copy-start | bytes 6291460
  6.5 64.3 %all-gather.6.cloned.1.call-start = ((), (), s32[]{:S(2)}) async-start(), calls=%async_computation.2 | async-start | bytes 1671168 | tf_op jit(solution)/shard_map/all_gather | solution.py:145
  9.6 120.7 %all-gather.8.cloned.1.call-start = ((), (), s32[]{:S(2)}) async-start(), calls=%async_computation.3 | async-start | bytes 1671168 | tf_op jit(solution)/shard_map/all_gather | solution.py:146
  10.4 172.1 %reduce-scatter.3.cloned.1.call-start = ((), (), s32[]{:S(2)}) async-start(), calls=%async_computation.4 | async-start | bytes 1179648 | tf_op jit(solution)/shard_map/reduce_scatter | solution.py:151
  130.3 53.6 %copy-start.1 = (f32[2048]{0:T(1024)S(1)}, f32[2048]{0:T(1024)}, u32[]{:S(2)}) copy-start(f32[2048]{0:T(1024)} %param.20) | copy-start | bytes 24580
  175.4 152.2 %all-gather.10.cloned.1.call-start = ((), (), s32[]{:S(2)}) async-start(), calls=%async_computation.5 | async-start | bytes 12255232 | tf_op jit(solution)/shard_map/all_gather | solution.py:76
  176.0 293.9 %all-gather.12.cloned.1.call-start = ((), (), s32[]{:S(2)}) async-start(), calls=%async_computation.6 | async-start | bytes 12255232 | tf_op jit(solution)/shard_map/all_gather | solution.py:77
  176.6 476.1 %all-gather.14.cloned.1.call-start = ((), (), s32[]{:S(2)}) async-start(), calls=%async_computation.7 | async-start | bytes 12255232 | tf_op jit(solution)/shard_map/all_gather | solution.py:78
  177.2 495.9 %reduce-scatter.5.cloned.1.call-start = ((), (), s32[]{:S(2)}) async-start(), calls=%async_computation.8 | async-start | bytes 1179648 | tf_op jit(solution)/shard_map/reduce_scatter | solution.py:168
Sparse Core Ops, SparseCore 0:
  10.1 60.6 all-gather.5
  73.6 56.6 all-gather.7
  175.6 6.8 reduce-scatter.2
  185.1 142.5 all-gather.9
  330.2 139.5 all-gather.11
  472.4 180.2 all-gather.13
  666.7 6.3 reduce-scatter.4
where the time goes:
time: 685 us; the launch traced here: 684 us
  waiting for transfers between devices  589 us (86%)
  matrix products  45.1 us (7%)
  other arithmetic  16.4 us (2%)
  local copies, waits for them, and re-layouts  14.7 us (2%)
  between operations  13.7 us (2%)
    all_gather x1, waiting for transfers between devices, body(): lax.all_gather(down_weight, 'sp', axis=1, tiled=True)  183 us
    all_gather x1, waiting for transfers between devices, body(): lax.all_gather(gate_weight, 'sp', axis=0, tiled=True)  141 us
    all_gather x1, waiting for transfers between devices, body(): lax.all_gather(up_weight, 'sp', axis=0, tiled=True)  134 us
    all_gather x1, waiting for transfers between devices, body(): lax.all_gather(values, 'sp', axis=0, tiled=True)  59.5 us
    all_gather x1, waiting for transfers between devices, body(): lax.all_gather(key_turned, 'sp', axis=0, tiled=True)  57.5 us
    dot_general x1, matrix products, body(): terms = jnp.dot(hidden, down_full, preferred_element_type=jnp.float32)  13.8 us
  transfers between devices with their start and end apart: 7, of which 7 were waited for; matrix products, arithmetic and copies ran while one was open for 2% of the time, Pallas kernels for 0%

commit v1 on v0

--- a/solution.py
+++ b/solution.py
@@ -75,7 +75,7 @@
     gate_full, up_full, down_full = (
         lax.all_gather(gate_weight, "sp", axis=0, tiled=True),
         lax.all_gather(up_weight, "sp", axis=0, tiled=True),
-        lax.all_gather(down_weight, "sp", axis=1, tiled=True),
+        jnp.concatenate(lax.all_gather(down_weight, "sp"), axis=1),
     )
     places = lax.axis_index("sp") * own + jnp.arange(own, dtype=jnp.int32)
     grid_rows = places // GRID_W

time: 685 us -> 646 us (0.943)
  waiting for transfers between devices: 589 us -> 533 us
  local copies, waits for them, and re-layouts: 14.7 us -> 29.9 us
    all_gather x1, waiting for transfers between devices: 183 us -> 141 us  [body(): lax.all_gather(down_weight, 'sp')]
    reshape x0 -> x1, local copies, waits for them, and re-layouts: none -> 15.2 us  [body(): jnp.concatenate(lax.all_gather(down_weight, 'sp'), axis=1)]
    all_gather x1, waiting for transfers between devices: 141 us -> 127 us  [body(): lax.all_gather(gate_weight, 'sp', axis=0, tiled=True)]
  transfers between devices with their start and end apart: 7 -> 7, of which waited for: 7 -> 7; matrix products, arithmetic and copies ran while one was open for 2% -> 4% of each run, Pallas kernels for 0% -> 0%
where the time goes in v1:
time: 646 us; the launch traced here: 645 us
  waiting for transfers between devices  533 us (83%)
  matrix products  46.5 us (7%)
  local copies, waits for them, and re-layouts  29.9 us (5%)
  other arithmetic  16.4 us (3%)
  between operations  13.7 us (2%)
    all_gather x1, waiting for transfers between devices, body(): lax.all_gather(down_weight, 'sp')  141 us
    all_gather x1, waiting for transfers between devices, body(): lax.all_gather(up_weight, 'sp', axis=0, tiled=True)  134 us
    all_gather x1, waiting for transfers between devices, body(): lax.all_gather(gate_weight, 'sp', axis=0, tiled=True)  127 us
    all_gather x1, waiting for transfers between devices, body(): lax.all_gather(values, 'sp', axis=0, tiled=True)  59.5 us
    all_gather x1, waiting for transfers between devices, body(): lax.all_gather(key_turned, 'sp', axis=0, tiled=True)  57.5 us
    dot_general x1, matrix products, body(): terms = jnp.dot(hidden, down_full, preferred_element_type=jnp.float32)  15.2 us
    reshape x1, local copies, waits for them, and re-layouts, body(): jnp.concatenate(lax.all_gather(down_weight, 'sp'), axis=1)  15.2 us
  transfers between devices with their start and end apart: 7, of which 7 were waited for; matrix products, arithmetic and copies ran while one was open for 4% of the time, Pallas kernels for 0%

profile of v1, /device:TPU:0, one launch (start us, length us, event | category | flops | bytes accessed | tf_op | source)
XLA Modules:
  0.0 645.1 jit_solution(5440576227658186768)
XLA Ops:
  6.6 1.1 copy.28
  7.8 0.8 fusion.22
  8.6 0.2 multiply_cosine_fusion.1
  8.8 0.7 copy.29
  9.6 0.0 all-gather.9.cloned.1.call-start
  9.7 0.7 all-gather.9.cloned.1.call-update
  10.4 0.0 reduce-scatter.3.cloned.1.call-start
  10.4 1.1 copy.30
  11.5 0.1 fusion.19
  11.6 0.8 fusion.20
  12.4 0.1 subtract_convert_fusion.1
  12.5 0.7 pad_maximum_fusion
  13.3 57.5 %all-gather.7.cloned.1.call-done = bf16[3072,256]{1,0:T(8,128)(2,1)} async-done(((bf16[192,256]{1,0:T(8,128)(2,1)}), bf16[3072,256]{1,0:T(8,128)(2,1)}) %all-gather.7.cloned.1.call-update) | async-done | bytes 1572880 | tf_op jit(solution)/shard_map/all_gather | solution.py:145
  70.8 59.5 %all-gather.9.cloned.1.call-done = bf16[3072,256]{1,0:T(8,128)(2,1)} async-done(((bf16[192,256]{1,0:T(8,128)(2,1)}), bf16[3072,256]{1,0:T(8,128)(2,1)}) %all-gather.9.cloned.1.call-update) | async-done | bytes 1572880 | tf_op jit(solution)/shard_map/all_gather | solution.py:146
  130.3 43.6 %while.15 = (s32[]{:T(128)}, f32[192,4,2]{0,2,1:T(2,128)S(1)}, f32[192,4,2]{0,2,1:T(2,128)S(1)}, f32[192,4,2,64]{0,3,2,1:T(8,128)S(1)}, bf16[2,1536,256]{2,1,0:T...) while((s32[]{:T(128)}, f32[192,4,2]{0,2,1:T(2,128)S(1)}, ...), condition=%wide.region_5.6_spmd.clone, body=%wide.region_2.5_spmd.clone.sunk | while | flops 623156736 | bytes 37257324 | solution.py:134
  130.3 2.6 constant_dynamic-slice_fusion.3
  132.9 1.4 copy.40
  134.3 6.0 bitcast_reduce_fusion.2
  140.4 5.4 fusion.51
  145.8 1.4 copy.41
  147.2 4.8 fusion.53
  152.1 2.6 constant_dynamic-slice_fusion.3
  154.7 1.4 copy.40
  156.1 6.0 bitcast_reduce_fusion.2
  162.1 5.4 fusion.51
  167.6 1.4 copy.41
  169.0 4.8 fusion.53
  173.9 0.1 divide_convert_fusion
  173.9 1.5 convolution_convert_fusion.1
  175.4 0.0 all-gather.15.cloned.1.call-start
  175.5 0.5 all-gather.15.cloned.1.call-update
  176.1 0.5 all-gather.11.cloned.1.call-update
  176.7 0.5 all-gather.13.cloned.1.call-update
  177.2 0.0 reduce-scatter.5.cloned.1.call-start
  177.2 5.2 reduce-scatter.3.cloned.1.call-done
  182.5 1.4 fusion.15
  183.9 0.2 fusion.17
  184.0 2.5 all_gather.26
  186.6 141.1 %all-gather.15.cloned.1.call-done = bf16[45056,128]{1,0:T(8,128)(2,1)} async-done(((bf16[2816,128]{1,0:T(8,128)(2,1)}), bf16[45056,128]{1,0:T(8,128)(2,1)}) %all-gather.15.cloned.1.call-update) | async-done | bytes 11534352 | tf_op jit(solution)/shard_map/all_gather | solution.py:78
  327.6 15.2 %copy.33 = bf16[2816,16,128]{0,2,1:T(8,128)(2,1)} copy(bf16[2816,16,128]{2,0,1:T(8,128)(2,1)} %bitcast.78) | data formatting | bytes 23068672 | tf_op jit(solution)/shard_map/reshape | solution.py:78
  342.8 127.1 %all-gather.11.cloned.1.call-done = bf16[2048,2816]{1,0:T(8,128)(2,1)} async-done(((bf16[128,2816]{1,0:T(8,128)(2,1)}), bf16[2048,2816]{1,0:T(8,128)(2,1)}) %all-gather.11.cloned.1.call-update) | async-done | bytes 11534352 | tf_op jit(solution)/shard_map/all_gather | solution.py:76
  469.9 8.0 %fusion.27 = f32[192,2816]{1,0:T(8,128)} fusion(bf16[192,2048]{1,0:T(8,128)(2,1)S(1)} %all_gather.26, bf16[2048,2816]{1,0:T(8,128)(2,1)} %all-gather.11.cloned.1.call-done), kind=kOutput, calls=%fused_computation.67 | convolution fusion | flops 2214592512 | bytes 14483456 | tf_op jit(solution)/shard_map/dot_general | solution.py:164
  477.9 134.2 %all-gather.13.cloned.1.call-done = bf16[2048,2816]{1,0:T(8,128)(2,1)} async-done(((bf16[128,2816]{1,0:T(8,128)(2,1)}), bf16[2048,2816]{1,0:T(8,128)(2,1)}) %all-gather.13.cloned.1.call-update) | async-done | bytes 11534352 | tf_op jit(solution)/shard_map/all_gather | solution.py:77
  612.1 15.2 %convolution_convert_fusion = bf16[192,2048]{1,0:T(8,128)(2,1)} fusion(bf16[2816,2048]{0,1:T(8,128)(2,1)} %bitcast.79, bf16[192,2048]{1,0:T(8,128)(2,1)S(1)} %all_gather.26, bf16[2048,2816]{1,0:T(8,128)(2,1)} %all-gather.13.cloned.1.call-done, f32[192,2816]{1,0:T(8,128)} %fusion.27), kind=kOutput, calls=%fused_computation.19 | convolution fusion | flops 4432822272 | bytes 26804224 | tf_op jit(solution)/shard_map/dot_general | solution.py:167
  627.4 6.5 %reduce-scatter.5.cloned.1.call-done = bf16[96,2048]{1,0:T(8,128)(2,1)} async-done(((bf16[192,2048]{1,0:T(8,128)(2,1)}), bf16[96,2048]{1,0:T(8,128)(2,1)}) %reduce-scatter.5.cloned.1.call-update) | async-done | bytes 393232 | tf_op jit(solution)/shard_map/reduce_scatter | solution.py:168
  633.9 1.1 fusion.18
  635.0 2.4 all_gather.31
  637.3 0.9 copy.55
  (27 shorter events, 0.4 us)
Async XLA Ops:
  6.5 167.4 %copy-start = (bf16[512,2048]{1,0:T(8,128)(2,1)S(1)}, bf16[512,2048]{1,0:T(8,128)(2,1)}, u32[]{:S(2)}) copy-start(bf16[512,2048]{1,0:T(8,128)(2,1)} %param.18) | copy-start | bytes 6291460
  6.5 64.3 %all-gather.7.cloned.1.call-start = ((), (), s32[]{:S(2)}) async-start(), calls=%async_computation.2 | async-start | bytes 1671168 | tf_op jit(solution)/shard_map/all_gather | solution.py:145
  9.6 120.7 %all-gather.9.cloned.1.call-start = ((), (), s32[]{:S(2)}) async-start(), calls=%async_computation.3 | async-start | bytes 1671168 | tf_op jit(solution)/shard_map/all_gather | solution.py:146
  10.4 172.1 %reduce-scatter.3.cloned.1.call-start = ((), (), s32[]{:S(2)}) async-start(), calls=%async_computation.4 | async-start | bytes 1179648 | tf_op jit(solution)/shard_map/reduce_scatter | solution.py:151
  130.3 53.6 %copy-start.1 = (f32[2048]{0:T(1024)S(1)}, f32[2048]{0:T(1024)}, u32[]{:S(2)}) copy-start(f32[2048]{0:T(1024)} %param.20) | copy-start | bytes 24580
  175.4 152.2 %all-gather.15.cloned.1.call-start = ((), (), s32[]{:S(2)}) async-start(), calls=%async_computation.8 | async-start | bytes 12255232 | tf_op jit(solution)/shard_map/all_gather | solution.py:78
  176.0 293.9 %all-gather.11.cloned.1.call-start = ((), (), s32[]{:S(2)}) async-start(), calls=%async_computation.5 | async-start | bytes 12255232 | tf_op jit(solution)/shard_map/all_gather | solution.py:76
  176.6 435.5 %all-gather.13.cloned.1.call-start = ((), (), s32[]{:S(2)}) async-start(), calls=%async_computation.6 | async-start | bytes 12255232 | tf_op jit(solution)/shard_map/all_gather | solution.py:77
  177.2 456.7 %reduce-scatter.5.cloned.1.call-start = ((), (), s32[]{:S(2)}) async-start(), calls=%async_computation.7 | async-start | bytes 1179648 | tf_op jit(solution)/shard_map/reduce_scatter | solution.py:168
Sparse Core Ops, SparseCore 0:
  10.1 60.6 all-gather.6
  73.6 56.6 all-gather.8
  175.6 6.8 reduce-scatter.2
  185.1 142.5 all-gather.14
  330.2 139.5 all-gather.10
  472.5 139.5 all-gather.12
  627.5 6.3 reduce-scatter.4
